TPU v7x, 32 devices: a whole 2x2x4 slice. The times are simulated.
32 devices in a mesh: grp: 2 (over x), sp: 4 (over z), tp: 4 (over y, core).
Axes of the slice: x: 2, y: 2, z: 4, core: 2. Of those that a mesh axis runs over, the one named last changes fastest.
Arguments:
- prompt_layer_input: bfloat16 [24, 512, 2048], P('grp', 'sp'), parts along dimension 0, may hold values from -10 to 10
- next_token_input: bfloat16 [24, 2048], P('grp'), parts along dimension 0, may hold values from -6 to 6
- value_projection: bfloat16 [2048, 2048], P(None, 'tp'), may hold values from -0.125 to 0.125
- output_gate_matrix: bfloat16 [2048, 2048], P(None, 'tp'), may hold values from -0.125 to 0.125
- key_projection: bfloat16 [2048, 256], replicated, may hold values from -0.0390625 to 0.0390625
- query_projection: bfloat16 [2048, 256], replicated, may hold values from -0.125 to 0.125
- step_projection: bfloat16 [2048, 32], replicated, may hold values from -0.125 to 0.125
- value_filter_taps: bfloat16 [4, 2048], replicated, may hold values from -3 to 3
- key_filter_taps: bfloat16 [4, 256], replicated, may hold values from -3 to 3
- query_filter_taps: bfloat16 [4, 256], replicated, may hold values from -3 to 3
- step_size_bias: float32 [32], replicated, may hold values from -4.3 to -0.7
- head_decay_logarithm: float32 [32], replicated, may hold values from -8.5 to -0.5
- direct_path_weight: float32 [32], replicated, may hold values from 0.1 to 1.9
- gated_norm_gain: float32 [32, 64], replicated, may hold values from 0.1 to 1.9
- position_decay_offset: float32 [24, 512, 32], P('grp', 'sp'), parts along dimension 0, may hold values from -2.1 to 0
Outputs:
- state_cache: bfloat16 [24, 32, 64, 128], P('grp', 'tp', 'sp'), parts along dimension 0
- first_read: bfloat16 [24, 32, 64], P('grp', 'tp', 'sp'), parts along dimension 0
There are 2 independent parts, one for each index of `grp`. A program takes and returns all parts, laid end to end along the dimension named above; an argument that names none is the same for every part. Nothing has to cross between parts.
All inputs are finite; a program needn't handle non-finite values.
Results may differ from a plain program's by a relative error of at most 0.011.
Values may be sent and summed in bfloat16 or wider, within the bound.
A program may use at most 64 MiB of HBM per device.

v0:
```python
import jax
import jax.numpy as jnp
from jax import lax
from jax.sharding import PartitionSpec as P

HEADS = 32
P_SIZE = 64
GROUPS = 2
STATE = 128
CONV = 4
SPAN = 64


epsilon = 1e-06


def shifted(block, axis, distance):
    devices = range(lax.axis_size(axis))
    route = [(i - distance, i) for i in devices if i - distance in devices]
    return lax.ppermute(block, axis, route)


def broadcast(value, axis, source):
    kept = jnp.where(lax.axis_index(axis) == source, value, 0).astype(value.dtype)
    return lax.psum(kept, axis)


def prefix(shard, axis, combine, identity):
    length, here = (lax.axis_size(axis), lax.axis_index(axis))
    everything = lax.all_gather(shard, axis)
    start = jnp.broadcast_to(jnp.asarray(identity, shard.dtype), shard.shape)

    def lap(k, before):
        at = length - 1 - k
        reached = at > here
        new = combine(before, everything[at])
        return jnp.where(reached, new, before)

    return lax.fori_loop(0, length, lap, start)


def shards(
    prompt_layer_input,
    next_token_input,
    value_projection,
    output_gate_matrix,
    key_projection,
    query_projection,
    step_projection,
    value_filter_taps,
    key_filter_taps,
    query_filter_taps,
    step_size_bias,
    head_decay_logarithm,
    direct_path_weight,
    gated_norm_gain,
    position_decay_offset,
):
    seq_count, local_len, width = prompt_layer_input.shape
    resident_heads = value_projection.shape[1] // P_SIZE
    feature_cols = resident_heads * P_SIZE
    shard_count = lax.axis_size("sp")
    rows_here = P_SIZE // shard_count
    shard_index = lax.axis_index("sp")
    leading_head = lax.axis_index("tp") * resident_heads
    group_index = leading_head // (HEADS // GROUPS)
    row_first = shard_index * rows_here
    in_cols = lax.dynamic_slice_in_dim(key_projection, group_index * STATE, STATE, 1)
    out_cols = lax.dynamic_slice_in_dim(query_projection, group_index * STATE, STATE, 1)
    weights_here = jnp.concatenate([value_projection, in_cols, out_cols], axis=1)
    step_cols = lax.dynamic_slice_in_dim(step_projection, leading_head, resident_heads, 1)
    kernel = jnp.concatenate(
        [
            lax.dynamic_slice_in_dim(value_filter_taps, leading_head * P_SIZE, feature_cols, 1),
            lax.dynamic_slice_in_dim(key_filter_taps, group_index * STATE, STATE, 1),
            lax.dynamic_slice_in_dim(query_filter_taps, group_index * STATE, STATE, 1),
        ],
        axis=1,
    ).astype(jnp.float32)
    head_decay_speed = jnp.exp(
        lax.dynamic_slice_in_dim(head_decay_logarithm, leading_head, resident_heads, 0)
    )
    bias_here = lax.dynamic_slice_in_dim(step_size_bias, leading_head, resident_heads, 0)
    skip_here = lax.dynamic_slice_in_dim(direct_path_weight, leading_head, resident_heads, 0)
    gain_here = lax.dynamic_slice(
        gated_norm_gain, (leading_head, row_first), (resident_heads, rows_here)
    )
    token_rows = prompt_layer_input.reshape(seq_count * local_len, width)
    projected = jnp.dot(token_rows, weights_here, preferred_element_type=jnp.float32).astype(
        jnp.bfloat16
    )
    projected = projected.reshape(seq_count, local_len, feature_cols + 2 * STATE)
    trailing = projected[:, local_len - (CONV - 1) :]
    before = shifted(trailing, "sp", 1)
    newest = broadcast(trailing, "sp", shard_count - 1)
    padded = jnp.concatenate([before, projected], axis=1)
    total = padded[:, 0:local_len].astype(jnp.float32) * kernel[0]
    for tap in range(1, CONV):
        total = total + padded[:, tap : tap + local_len].astype(jnp.float32) * kernel[tap]
    mixed = jax.nn.silu(total).astype(jnp.bfloat16)
    step_raw = jnp.dot(token_rows, step_cols, preferred_element_type=jnp.float32).astype(
        jnp.bfloat16
    )
    discrete_step = jax.nn.softplus(step_raw.astype(jnp.float32) + bias_here).reshape(
        seq_count, local_len, resident_heads
    )
    decay_spikes = lax.dynamic_slice_in_dim(position_decay_offset, leading_head, resident_heads, 2)
    logarithmic_decay = decay_spikes - head_decay_speed * discrete_step
    block_count = local_len // SPAN
    cumulative = jnp.cumsum(
        logarithmic_decay.reshape(seq_count, block_count, SPAN, resident_heads), axis=2
    )
    decay_weight = jnp.exp(cumulative[:, :, -1:] - cumulative) * discrete_step.reshape(
        seq_count, block_count, SPAN, resident_heads
    )
    head_input = mixed[:, :, :feature_cols].reshape(
        seq_count, block_count, SPAN, resident_heads, P_SIZE
    )
    weighted = (head_input.astype(jnp.float32) * decay_weight[..., None]).astype(jnp.bfloat16)
    in_map = mixed[:, :, feature_cols : feature_cols + STATE].reshape(
        seq_count, block_count, SPAN, STATE
    )
    block_state = jnp.einsum(
        "bcshp,bcsn->bchpn", weighted, in_map, preferred_element_type=jnp.float32
    )
    block_log = cumulative[:, :, -1]
    own_log = jnp.sum(block_log, axis=1)
    after_block = jnp.exp(own_log[:, None] - jnp.cumsum(block_log, axis=1))
    local_state = jnp.sum(after_block[..., None, None] * block_state, axis=1)
    later_log = prefix(own_log, "sp", jnp.add, jnp.zeros_like(own_log))
    scaled = jnp.exp(later_log)[:, :, None, None] * local_state
    own_rows = lax.psum_scatter(scaled, "sp", scatter_dimension=2, tiled=True)
    state_cache = own_rows.astype(jnp.bfloat16)
    new_raw = jnp.dot(next_token_input, weights_here, preferred_element_type=jnp.float32).astype(
        jnp.bfloat16
    )
    new_step = jnp.dot(next_token_input, step_cols, preferred_element_type=jnp.float32).astype(
        jnp.bfloat16
    )
    new_gate = jnp.dot(
        next_token_input, output_gate_matrix, preferred_element_type=jnp.float32
    ).astype(jnp.bfloat16)
    window = jnp.concatenate([newest, new_raw[:, None]], axis=1)
    new_mixed = jax.nn.silu(jnp.sum(window.astype(jnp.float32) * kernel[None], axis=1)).astype(
        jnp.bfloat16
    )
    new_input = lax.dynamic_slice_in_dim(
        new_mixed[:, :feature_cols].reshape(seq_count, resident_heads, P_SIZE),
        row_first,
        rows_here,
        2,
    ).astype(jnp.float32)
    new_in = new_mixed[:, feature_cols : feature_cols + STATE].astype(jnp.float32)
    new_out = new_mixed[:, feature_cols + STATE :].astype(jnp.float32)
    new_step_size = jax.nn.softplus(new_step.astype(jnp.float32) + bias_here)
    cache_values = lax.optimization_barrier(state_cache).astype(jnp.float32)
    new_state = (
        jnp.exp(-head_decay_speed * new_step_size)[:, :, None, None] * cache_values
        + (new_step_size[:, :, None] * new_input)[..., None] * new_in[:, None, None, :]
    )
    readout = (
        jnp.sum(new_state * new_out[:, None, None, :], axis=-1)
        + skip_here[None, :, None] * new_input
    )
    gate_rows = lax.dynamic_slice_in_dim(
        new_gate.reshape(seq_count, resident_heads, P_SIZE), row_first, rows_here, 2
    )
    gated = readout * jax.nn.silu(gate_rows.astype(jnp.float32))
    squares = lax.psum(jnp.sum(gated * gated, axis=(1, 2)), ("sp", "tp"))
    scale = lax.rsqrt(squares / (HEADS * P_SIZE) + epsilon)
    first_read = (gated * scale[:, None, None] * gain_here[None]).astype(jnp.bfloat16)
    return (state_cache, first_read)


def solution(mesh):
    in_specs = (
        P("grp", "sp", None),
        P("grp", None),
        P(None, "tp"),
        P(None, "tp"),
        P(),
        P(),
        P(),
        P(),
        P(),
        P(),
        P(),
        P(),
        P(),
        P(),
        P("grp", "sp", None),
    )
    out_specs = (P("grp", "tp", "sp", None), P("grp", "tp", "sp"))
    return jax.shard_map(shards, mesh=mesh, in_specs=in_specs, out_specs=out_specs, check_vma=False)
```

profile of v0, /device:TPU:0, one launch (start us, length us, event | category | flops | bytes accessed | tf_op | source)
XLA Modules:
  0.0 183.3 jit_solution(16394468105042991492)
XLA Ops:
  7.2 1.4 constant_dynamic-slice_fusion.3
  8.7 0.8 copy-done.2
  9.5 0.2 copy-done.4
  9.6 8.9 %fusion.2 = bf16[1536,768]{0,1:T(8,128)(2,1)} fusion(bf16[1536,2048]{1,0:T(8,128)(2,1)} %bitcast.47, bf16[2048,128]{1,0:T(8,128)(2,1)S(1)} %get-tuple-element.156, bf16[2048,128]{1,0:T(8,128)(2,1)S(1)} %get-tuple-element.157, bf16[2048,512]{1,0:T(8,128)(2,1)} %param.19), kind=kOutput, calls=%fused_computation.10 | convolution fusion | flops 4842455040 | bytes 11796480 | tf_op jit(solution)/shard_map/dot_general | solution.py:89
  18.6 4.3 %copy.43 = bf16[1536,768]{1,0:T(8,128)(2,1)} copy(bf16[1536,768]{0,1:T(8,128)(2,1)} %fusion.2) | data formatting | bytes 4718592 | tf_op jit(solution)/shard_map/convert_element_type | solution.py:89
  22.9 1.0 broadcast_select_fusion
  23.9 5.0 %collective-permute-start = (bf16[12,3,768]{2,1,0:T(4,128)(2,1)S(1)}, bf16[12,3,768]{2,1,0:T(4,128)(2,1)S(1)}, u32[]{:S(2)}, u32[]{:S(2)}) collective-permute-start(bf16[12,3,768]{2,1,0:T(4,128)(2,1)S(1)} %get-tuple-element.145), channel_id=1, source_target_pairs={{0,4},{4,8},{8,12},{1,5},{5,9},{9,13},{2,6},{6,10},{10,14},{3,7},{... | collective-permute-start | bytes 165896 | tf_op jit(solution)/shard_map/ppermute | solution.py:20
  28.9 0.1 dynamic_slice.52
  29.0 4.6 %fusion.22 = (f32[12,128,8]{1,2,0:T(8,128)S(1)}, f32[1536,8]{0,1:T(8,128)S(1)}) fusion(f32[12,128,32]{1,2,0:T(8,128)} %param.31, s32[]{:T(128)S(6)} %select_n.75, f32[8]{0:T(128)S(1)} %get-tuple-element.143, f32[8]{0:T(128)S(1)} %dynamic_slice.52, bf16[1536,2048]{1,0:T(8,128)(2,1)} %bitcast.48, bf16[2048,32]{0,1:T(8,128)(2,1)} %param.23), kind=kOutput, calls=%fused_computation.45 | convolution fusion | flops 50466816 | bytes 6472768 | tf_op jit(solution)/shard_map/dot_general | solution.py:101
  33.6 0.1 reshape.87
  33.7 1.8 copy.39
  35.5 1.3 fusion.33
  36.8 0.6 slice_bitcast_fusion
  37.4 0.6 fusion.13
  38.0 0.1 copy.40
  38.1 0.1 reshape_reshape.3
  38.2 1.8 copy.44
  40.0 13.6 %all-gather.1 = f32[4,12,8]{1,2,0:T(8,128)S(1)} all-gather(f32[1,12,8]{1,2,0:T(8,128)S(1)} %bitcast.50), channel_id=2, replica_groups=mesh['grp'=2,'sp'=4,'tp'=4] {'sp'}, dimensions={0}, use_global_device_ids=true | all-gather | bytes 1920 | tf_op jit(solution)/shard_map/all_gather | solution.py:30
  53.6 0.1 while.16
  53.7 0.7 constant_dynamic-slice_fusion.2
  54.4 1.5 exponential_multiply_fusion
  56.0 0.5 copy.45
  56.4 0.6 copy.42
  57.0 0.1 copy.41
  57.1 7.3 %multiply_convert_fusion.1 = bf16[12,128,768]{2,1,0:T(8,128)(2,1)S(1)} fusion(bf16[12,128,768]{2,1,0:T(8,128)(2,1)} %bitcast.46, bf16[12,3,768]{2,1,0:T(4,128)(2,1)S(1)} %collective-permute-done, f32[768]{0:T(1024)S(1)} %get-tuple-element.129, f32[768]{0:T(1024)S(1)} %get-tuple-element.130, f32[768]{0:T(1024)S(1)} %get-tuple-element.131, ...), kind=kLoop, calls=%fused_computation.3 | loop fusion | flops 29491200 | bytes 4786176 | tf_op jit(solution)/shard_map/convert_element_type | solution.py:100
  64.5 2.1 %slice_convert_fusion = f32[12,128,512]{2,1,0:T(8,128)} fusion(bf16[12,128,768]{2,1,0:T(8,128)(2,1)S(1)} %multiply_convert_fusion.1), kind=kLoop, calls=%fused_computation.18 | loop fusion | flops 786432 | bytes 4718592 | tf_op jit(solution)/shard_map/convert_element_type | solution.py:119
  66.6 5.6 %reshape.92 = f32[12,2,64,8,64]{4,3,2,1,0:T(8,128)} reshape(f32[12,128,512]{2,1,0:T(8,128)} %slice_convert_fusion) | data formatting | bytes 6291456 | tf_op jit(solution)/shard_map/convert_element_type | solution.py:119
  72.2 4.4 %multiply_convert_fusion = bf16[12,2,64,8,64]{4,3,2,1,0:T(8,128)(2,1)S(1)} fusion(f32[12,2,64,8,64]{4,3,2,1,0:T(8,128)} %reshape.92, f32[12,2,64,8]{3,2,1,0:T(8,128)S(1)} %copy.45), kind=kLoop, calls=%fused_computation.2 | loop fusion | flops 1572864 | bytes 4767744 | tf_op jit(solution)/shard_map/convert_element_type | solution.py:119
  76.7 1.3 multiply_reduce_fusion
  78.1 1.9 %broadcast_multiply_fusion = f32[12,8,64,128]{3,2,1,0:T(8,128)} fusion(f32[12,8,64,128]{3,2,1,0:T(8,128)S(1)} %multiply_reduce_fusion, f32[12,8]{1,0:T(8,128)S(1)} %copy.41), kind=kLoop, calls=%fused_computation.19 | loop fusion | flops 786432 | bytes 6291840 | tf_op jit(solution)/shard_map/mul | solution.py:131
  80.0 0.1 dynamic_slice.59
  80.1 0.9 multiply_exponential_fusion
  81.0 0.1 copy.47
  81.1 0.1 copy.48
  81.2 0.4 convolution_convert_fusion.2
  81.6 0.1 reshape.91
  81.7 2.1 %fusion.12 = bf16[12,1,768]{2,0,1:T(8,128)(2,1)S(1)} fusion(bf16[12,2048]{1,0:T(8,128)(2,1)S(1)} %copy-done.6, bf16[2048,128]{1,0:T(8,128)(2,1)S(1)} %copy-done.3, bf16[2048,128]{1,0:T(8,128)(2,1)S(1)} %copy-done.5, bf16[2048,512]{1,0:T(8,128)(2,1)} %param.19), kind=kOutput, calls=%fused_computation.22 | convolution fusion | flops 47195136 | bytes 3213312 | tf_op jit(solution)/shard_map/dot_general | solution.py:134
  83.9 22.8 %psum.14 = bf16[12,3,768]{2,1,0:T(4,128)(2,1)S(1)} all-reduce(bf16[12,3,768]{2,1,0:T(4,128)(2,1)S(1)} %get-tuple-element.144), channel_id=1, replica_groups=mesh['grp'=2,'sp'=4,'tp'=4] {'sp'}, use_global_device_ids=true, to_apply=%region_7.8 | all-reduce | flops 27648 | bytes 110592 | tf_op jit(solution)/shard_map/psum | solution.py:25
  106.7 0.2 multiply_reduce_fusion.2
  106.9 0.1 reshape.90
  107.0 0.8 dynamic_slice.61
  107.8 0.1 convert_multiply_fusion.2
  107.9 33.7 %reduce-scatter.2.cloned.1.call-done = f32[12,8,16,128]{3,2,1,0:T(8,128)} async-done(((f32[12,8,64,128]{3,2,1,0:T(8,128)}), f32[12,8,16,128]{3,2,1,0:T(8,128)}) %reduce-scatter.2.cloned.1.call-update) | async-done | bytes 786448 | tf_op jit(solution)/shard_map/reduce_scatter | solution.py:132
  141.6 1.2 convert_element_type.104
  142.8 0.7 multiply_reduce_fusion.1
  143.5 0.3 multiply_reduce_fusion.3
  143.7 32.0 %psum.15 = f32[12]{0:T(128)S(1)} all-reduce(f32[12]{0:T(128)S(1)} %get-tuple-element.140), channel_id=1, replica_groups=mesh['grp'=2,'sp'=4,'tp'=4] {'sp','tp'}, use_global_device_ids=true, to_apply=%region_11.12 | all-reduce | flops 12 | bytes 96 | tf_op jit(solution)/shard_map/psum | solution.py:169
  175.8 0.7 multiply_convert_fusion.2
  (45 shorter events, 0.4 us)
Async XLA Ops:
  7.2 74.0 %copy-start = (bf16[2048,512]{1,0:T(8,128)(2,1)S(1)}, bf16[2048,512]{1,0:T(8,128)(2,1)}, u32[]{:S(2)}) copy-start(bf16[2048,512]{1,0:T(8,128)(2,1)} %param.20) | copy-start | bytes 6291460
  7.2 134.4 %reduce-scatter.2.cloned.1.call-start = ((), (), s32[]{:S(2)}) async-start(), calls=%async_computation.1 | async-start | bytes 3932160 | tf_op jit(solution)/shard_map/reduce_scatter | solution.py:132
  8.7 0.8 copy-start.2
  8.7 1.0 copy-start.4
  18.6 10.3 %copy-start.12 = (f32[32]{0:T(128)S(1)}, f32[32]{0:T(128)}, u32[]{:S(2)}) copy-start(f32[32]{0:T(128)} %param.27) | copy-start | bytes 388
  18.6 10.4 %copy-start.11 = (f32[32]{0:T(128)S(1)}, f32[32]{0:T(128)}, u32[]{:S(2)}) copy-start(f32[32]{0:T(128)} %param.28) | copy-start | bytes 388
  23.9 33.3 %collective-permute-start = (bf16[12,3,768]{2,1,0:T(4,128)(2,1)S(1)}, bf16[12,3,768]{2,1,0:T(4,128)(2,1)S(1)}, u32[]{:S(2)}, u32[]{:S(2)}) collective-permute-start(bf16[12,3,768]{2,1,0:T(4,128)(2,1)S(1)} %get-tuple-element.145), channel_id=1, source_target_pairs={{0,4},{4,8},{8,12},{1,5},{5,9},{9,13},{2,6},{6,10},{10,14},{3,7},{... | collective-permute-start | bytes 165896 | tf_op jit(solution)/shard_map/ppermute | solution.py:20
  29.0 24.7 %copy-start.9 = (bf16[4,256]{1,0:T(4,128)(2,1)S(1)}, bf16[4,256]{1,0:T(4,128)(2,1)}, u32[]{:S(2)}) copy-start(bf16[4,256]{1,0:T(4,128)(2,1)} %param.26) | copy-start | bytes 6148
  29.0 24.7 %copy-start.10 = (bf16[4,256]{1,0:T(4,128)(2,1)S(1)}, bf16[4,256]{1,0:T(4,128)(2,1)}, u32[]{:S(2)}) copy-start(bf16[4,256]{1,0:T(4,128)(2,1)} %param.25) | copy-start | bytes 6148
  38.2 18.2 %copy-start.7 = (f32[12,2,8]{2,0,1:T(8,128)S(1)}, f32[12,2,8]{2,0,1:T(8,128)}, u32[]{:S(2)}) copy-start(f32[12,2,8]{2,0,1:T(8,128)} %fusion.13) | copy-start | bytes 2308
  72.2 4.4 %copy-start.8 = (f32[12,2,8]{2,1,0:T(2,128)S(1)}, f32[12,2,8]{2,1,0:T(2,128)}, u32[]{:S(2)}) copy-start(f32[12,2,8]{2,1,0:T(2,128)} %copy.42) | copy-start | bytes 2308
  78.0 2.0 %copy-start.13 = (f32[32]{0:T(128)S(1)}, f32[32]{0:T(128)}, u32[]{:S(2)}) copy-start(f32[32]{0:T(128)} %param.29) | copy-start | bytes 388
  78.0 2.1 %copy-start.6 = (bf16[12,2048]{1,0:T(8,128)(2,1)S(1)}, bf16[12,2048]{1,0:T(8,128)(2,1)}, u32[]{:S(2)}) copy-start(bf16[12,2048]{1,0:T(8,128)(2,1)} %param.18) | copy-start | bytes 147460
  78.0 3.7 %copy-start.3 = (bf16[2048,128]{1,0:T(8,128)(2,1)S(1)}, bf16[2048,128]{1,0:T(8,128)(2,1)}, u32[]{:S(2)}) copy-start(bf16[2048,128]{1,0:T(8,128)(2,1)} %copy-done.2) | copy-start | bytes 1572868
  78.1 3.7 %copy-start.5 = (bf16[2048,128]{1,0:T(8,128)(2,1)S(1)}, bf16[2048,128]{1,0:T(8,128)(2,1)}, u32[]{:S(2)}) copy-start(bf16[2048,128]{1,0:T(8,128)(2,1)} %copy-done.4) | copy-start | bytes 1572868
  142.8 33.7 %copy-start.1 = (bf16[12,8,16,128]{3,2,1,0:T(8,128)(2,1)}, bf16[12,8,16,128]{3,2,1,0:T(8,128)(2,1)S(1)}, u32[]{:S(2)}) copy-start(bf16[12,8,16,128]{3,2,1,0:T(8,128)(2,1)S(1)} %convert_element_type.104) | copy-start | bytes 1179652
Sparse Core Ops, SparseCore 0:
  80.2 61.3 reduce-scatter.1
where the time goes:
time: 184 us; the launch traced here: 183 us
  blocking collectives  68.4 us (37%)
  waiting for transfers between devices  33.7 us (18%)
  other arithmetic  24 us (13%)
  local copies, waits for them, and re-layouts  19.5 us (11%)
  matrix products  18.2 us (10%)
  between operations  14.4 us (8%)
  starting transfers between devices  5.01 us (3%)
    reduce_scatter x1, waiting for transfers between devices, shards(): own_rows = lax.psum_scatter(scaled, 'sp', scatter_dimension=2, tiled=True)  33.7 us
    psum x1, blocking collectives, shards(): squares = lax.psum(jnp.sum(gated * gated, axis=(1, 2)), ('sp', 'tp'))  32 us
    psum x1, blocking collectives, broadcast(): return lax.psum(kept, axis)  22.8 us
    all_gather x1, blocking collectives, prefix(): everything = lax.all_gather(shard, axis)  13.6 us
    dot_general x1, matrix products, shards(): jnp.dot(token_rows, weights_here, preferred_element_type=jnp.float32)  8.94 us
    convert_element_type x1, other arithmetic, shards(): mixed = jax.nn.silu(total).astype(jnp.bfloat16)  7.27 us
    convert_element_type x1, local copies, waits for them, and re-layouts, shards(): head_input.astype(jnp.float32) * decay_weight[..., None]  5.6 us
    ppermute x1, starting transfers between devices, shifted(): return lax.ppermute(block, axis, route)  4.97 us
  transfers between devices with their start and end apart: 2, of which 1 were waited for; matrix products, arithmetic and copies ran while one was open for 11% of the time, Pallas kernels for 0%

commit v1 on v0

--- a/solution.py
+++ b/solution.py
@@ -1,6 +1,8 @@
 import jax
 import jax.numpy as jnp
 from jax import lax
+from jax.experimental import pallas as pl
+from jax.experimental.pallas import tpu as pltpu
 from jax.sharding import PartitionSpec as P
 
 HEADS = 32
@@ -172,6 +174,435 @@
     return (state_cache, first_read)
 
 
+F32, BF16 = jnp.float32, jnp.bfloat16
+MESH = pl.DeviceIdType.MESH
+EXACT = lax.Precision.HIGHEST
+
+
+def exact_dot(a, b, dims=((1,), (0,))):
+    return lax.dot_general(a, b, (dims, ((), ())), precision=EXACT, preferred_element_type=F32)
+
+
+def softplus(v):
+    return jnp.maximum(v, 0.0) + jnp.log1p(jnp.exp(-jnp.abs(v)))
+
+
+def silu(v):
+    return v / (1.0 + jnp.exp(-v))
+
+
+def ones_where(shape, test, dtype=F32):
+    rows = lax.broadcasted_iota(jnp.int32, shape, 0)
+    cols = lax.broadcasted_iota(jnp.int32, shape, 1)
+    return jnp.where(test(rows, cols), 1.0, 0.0).astype(dtype)
+
+
+def mixer_kernel(
+    dims,
+    x_hbm,
+    next_ref,
+    wv_hbm,
+    wg_hbm,
+    wk_hbm,
+    wq_hbm,
+    ws_hbm,
+    tv_ref,
+    tk_ref,
+    tq_ref,
+    bias_ref,
+    speed_ref,
+    skip_ref,
+    gain_ref,
+    off_hbm,
+    cache_ref,
+    read_ref,
+    xbuf,
+    edge,
+    wall,
+    wq,
+    ws,
+    wg,
+    off,
+    taps,
+    pad,
+    halo_out,
+    halo_in,
+    halo,
+    newest,
+    logs_out,
+    logs,
+    sendbuf,
+    recv,
+    sq_out,
+    sq_in,
+    expand,
+    load_sem,
+    x_sem,
+    halo_sem,
+    new_send,
+    new_recv,
+    st_send,
+    st_recv,
+    log_send,
+    log_recv,
+    sq_send,
+    sq_recv,
+):
+    n, m, S, L, heads, R, G = dims
+    F = heads * P_SIZE
+    C = F + STATE
+    SP = sq_out.shape[0]
+    steps = S // G
+    me, tp = lax.axis_index("sp"), lax.axis_index("tp")
+    lead = tp * heads
+    group = lax.div(lead, HEADS // GROUPS)
+    fcol = pl.multiple_of(tp * F, 128)
+    gcol = pl.multiple_of(group * STATE, 128)
+
+    def load(src, dst, k):
+        c = pltpu.make_async_copy(src, dst, load_sem.at[k])
+        c.start()
+        return c
+
+    def load_x(g):
+        return pltpu.make_async_copy(
+            x_hbm.at[pl.ds(g * G, G)], xbuf.at[pl.ds(g * G, G)], x_sem.at[g]
+        )
+
+    first = [
+        load(x_hbm.at[:, pl.ds(L - 16, 16)], edge.at[pl.ds(0, S)], 0),
+        load(wk_hbm.at[:, pl.ds(gcol, STATE)], wall.at[:, pl.ds(F, STATE)], 1),
+        load(ws_hbm, ws, 2),
+        load(wq_hbm.at[:, pl.ds(gcol, STATE)], wq, 3),
+        load(wv_hbm, wall.at[:, pl.ds(0, F)], 4),
+    ]
+    for g in range(steps):
+        load_x(g).start()
+    off_load = load(off_hbm, off, 5)
+    gate_load = load(wg_hbm, wg, 6)
+
+    peers = [(a, b) for a in range(n) for b in range(m) if (a, b) != (0, 0)]
+
+    def at(a, b=0):
+        return {"sp": lax.rem(me + a, n), "tp": lax.rem(tp + b, m)}
+
+    barrier = pltpu.get_barrier_semaphore()
+    for a, b in peers:
+        pl.semaphore_signal(barrier, inc=1, device_id=at(a, b), device_id_type=MESH)
+
+    taps[:, 0:F] = tv_ref[:, pl.ds(fcol, F)].astype(F32)
+    taps[:, F:C] = tk_ref[:, pl.ds(gcol, STATE)].astype(F32)
+    taps[:, C : C + STATE] = tq_ref[:, pl.ds(gcol, STATE)].astype(F32)
+    edge[S] = jnp.zeros(edge.shape[1:], BF16)
+    edge[S, 0:S, :] = next_ref[...]
+    logs_out[...] = jnp.zeros_like(logs_out)
+    halo_out[...] = jnp.zeros_like(halo_out)
+    newest_zero = jnp.zeros(newest.shape[1:], F32)
+    head_of = ones_where((HEADS, F), lambda i, c: i == lead + lax.div(c, P_SIZE), BF16)
+    expand[0:HEADS, :] = head_of
+    expand[HEADS : 2 * HEADS, :] = head_of
+    bias = bias_ref[...]
+    speed = jnp.exp(speed_ref[...])
+
+    for c in first:
+        c.wait()
+    wall[:, C : C + STATE] = jnp.concatenate(
+        [ws[...], jnp.zeros((ws.shape[0], STATE - HEADS), BF16)], axis=1
+    )
+    rows = edge[...].reshape((S + 1) * 16, edge.shape[2])
+    eproj = jnp.dot(rows, wall[...], preferred_element_type=F32).astype(BF16).astype(F32)
+    eq = jnp.dot(rows, wq[...], preferred_element_type=F32).astype(BF16).astype(F32)
+    e3 = eproj.reshape(S + 1, 16, C + STATE)
+    q3 = eq.reshape(S + 1, 16, STATE)
+    total = jnp.zeros((S, C + STATE), F32)
+    for j in range(CONV - 1):
+        row = 16 - (CONV - 1) + j
+        tail = e3[0:S, row, 0:C]
+        halo_out[j, 0:S, :] = tail.astype(BF16)
+        total = total + jnp.concatenate([tail, q3[0:S, row, :]], axis=1) * taps[j : j + 1, :]
+    new_raw = jnp.concatenate([e3[S, :, 0:C], q3[S]], axis=1)
+    new_step = e3[S, :, C : C + HEADS]
+
+    pl.semaphore_wait(barrier, len(peers))
+
+    def halo_copy():
+        return pltpu.make_async_remote_copy(
+            halo_out, halo_in, halo_sem.at[0], halo_sem.at[1], device_id=at(1), device_id_type=MESH
+        )
+
+    @pl.when(me < n - 1)
+    def _():
+        halo_copy().start()
+
+    def newest_copy(k):
+        return pltpu.make_async_remote_copy(
+            newest, newest, new_send.at[k], new_recv, device_id=at(k), device_id_type=MESH
+        )
+
+    @pl.when(me == n - 1)
+    def _():
+        newest[0] = newest_zero
+        newest[0, 0:S, :] = total
+        for k in range(1, n):
+            newest_copy(k).start()
+
+    def state_copy(g, k):
+        to = lax.rem(me + k, n)
+        return pltpu.make_async_remote_copy(
+            sendbuf.at[to, pl.ds(g * G, G)],
+            recv.at[me, pl.ds(g * G, G)],
+            st_send.at[g, k],
+            st_recv.at[g, k],
+            device_id=at(k),
+            device_id_type=MESH,
+        )
+
+    off_load.wait()
+    later_ones = ones_where((L, L), lambda t, u: u > t)
+
+    def step(g, carry):
+        load_x(g).wait()
+        xg = xbuf[pl.ds(g * G, G)].reshape(G * L, xbuf.shape[2])
+        acc = jnp.dot(xg, wall[...], preferred_element_type=F32).astype(BF16).astype(F32)
+
+        @pl.when(g == 0)
+        def _():
+            @pl.when(me == 0)
+            def _():
+                halo[...] = jnp.zeros_like(halo)
+
+            @pl.when(me > 0)
+            def _():
+                halo_copy().wait_recv()
+                halo[...] = halo_in[...].astype(F32)
+
+        for q in range(G):
+            p = g * G + q
+            raw = acc[q * L : (q + 1) * L]
+            pad[q, 8 : 8 + L, :] = raw[:, 0:C]
+            for j in range(CONV - 1):
+                r = 8 - (CONV - 1) + j
+                pad[q, r : r + 1, :] = halo[j, pl.ds(p, 1), :]
+            dt = softplus(raw[:, C : C + HEADS] + bias)
+            ld = off[p] - speed * dt
+            suffix = exact_dot(later_ones, ld)
+            logs_out[pl.ds(p, 1), 0:HEADS] = suffix[0:1] + ld[0:1]
+            w = dt * jnp.exp(suffix)
+            hi = w.astype(BF16)
+            lo = (w - hi.astype(F32)).astype(BF16)
+            wide = jnp.dot(
+                jnp.concatenate([hi, lo], axis=1), expand[...], preferred_element_type=F32
+            )
+
+            def mixed(c):
+                s = slice(c, c + 128)
+                t = pad[q, 8 - (CONV - 1) : 8 - (CONV - 1) + L, s] * taps[0:1, s]
+                for j in range(1, CONV):
+                    r = 8 - (CONV - 1) + j
+                    t = t + pad[q, r : r + L, s] * taps[j : j + 1, s]
+                return silu(t).astype(BF16)
+
+            in_map = mixed(F)
+            for c in range(0, F, 128):
+                weighted = (mixed(c).astype(F32) * wide[:, c : c + 128]).astype(BF16)
+                share = lax.dot_general(
+                    weighted, in_map, (((0,), (0,)), ((), ())), preferred_element_type=F32
+                ).astype(BF16)
+                for hh in range(128 // P_SIZE):
+                    h = c // P_SIZE + hh
+                    for d in range(n):
+                        b = hh * P_SIZE + d * R
+                        sendbuf[d, p, h * R : (h + 1) * R, :] = share[b : b + R]
+        for k in range(1, n):
+            state_copy(g, k).start()
+        return carry
+
+    lax.fori_loop(0, steps, step, 0)
+
+    def log_copy(k):
+        return pltpu.make_async_remote_copy(
+            logs_out, logs.at[me], log_send.at[k], log_recv.at[k], device_id=at(k), device_id_type=MESH
+        )
+
+    for k in range(1, n):
+        log_copy(k).start()
+    logs[me] = logs_out[...]
+    recv[me] = sendbuf[me]
+
+    RH = heads * R
+    head_rows = ones_where((RH, HEADS), lambda l, i: i == lead + lax.div(l, R))
+    head_cols = ones_where((HEADS, RH), lambda i, l: i == lead + lax.div(l, R))
+    pick = ones_where(
+        (F, RH), lambda c, l: c == lax.div(l, R) * P_SIZE + me * R + lax.rem(l, R), BF16
+    )
+    row_pick = ones_where((P_SIZE, RH), lambda c, l: c == me * R + lax.rem(l, R))
+    gate_load.wait()
+    gate = jnp.dot(edge[S], wg[...], preferred_element_type=F32).astype(BF16)
+    gate_here = silu(jnp.dot(gate, pick, preferred_element_type=F32))
+    gain_here = jnp.sum(exact_dot(gain_ref[...], row_pick) * head_cols, axis=0, keepdims=True)
+    skip_here = exact_dot(skip_ref[...], head_cols)
+    new_dt = softplus(new_step + bias)
+    dt_here = exact_dot(new_dt, head_cols)
+    keep_here = jnp.exp(-exact_dot(speed * new_dt, head_cols))
+
+    @pl.when(me < n - 1)
+    def _():
+        pltpu.make_async_remote_copy(
+            newest, newest, new_send.at[0], new_recv, device_id=at(1), device_id_type=MESH
+        ).wait_recv()
+
+    new_mixed = silu(newest[0] + new_raw * taps[CONV - 1 : CONV, :]).astype(BF16)
+    new_input = jnp.dot(new_mixed[:, 0:F], pick, preferred_element_type=F32)
+    new_in = new_mixed[:, F:C].astype(F32)
+    new_out = new_mixed[:, C : C + STATE]
+    both = jnp.sum(new_in * new_out.astype(F32), axis=1, keepdims=True)
+
+    for k in range(1, n):
+        log_copy(k).wait_recv()
+    later = jnp.zeros(logs_out.shape, F32)
+    factors = [None] * n
+    for s in reversed(range(n)):
+        factors[s] = exact_dot(head_rows, jnp.exp(later)[:, 0:HEADS], ((1,), (1,)))
+        later = later + logs[s]
+
+    where_row = lax.broadcasted_iota(jnp.int32, (SP, RH), 0)
+    y = jnp.zeros((SP, RH), F32)
+    for g in range(steps):
+        for k in range(1, n):
+            state_copy(g, k).wait_recv()
+        for p in range(g * G, (g + 1) * G):
+            tot = factors[0][:, p : p + 1] * recv[0, p].astype(F32)
+            for s in range(1, n):
+                tot = tot + factors[s][:, p : p + 1] * recv[s, p].astype(F32)
+            kept = tot.astype(BF16)
+            cache_ref[p] = kept
+            part = lax.dot_general(
+                new_out, kept, (((1,), (1,)), ((), ())), preferred_element_type=F32
+            )
+            y = jnp.where(where_row == p, part, y)
+    readout = keep_here * y + dt_here * new_input * both + skip_here * new_input
+    gated = readout * gate_here
+    sq = jnp.broadcast_to(jnp.sum(gated * gated, axis=1, keepdims=True), sq_out.shape)
+    sq_out[...] = sq
+
+    def sq_copy(i):
+        a, b = peers[i]
+        return pltpu.make_async_remote_copy(
+            sq_out, sq_in.at[i], sq_send.at[i], sq_recv.at[i], device_id=at(a, b), device_id_type=MESH
+        )
+
+    for i in range(len(peers)):
+        sq_copy(i).start()
+    for i in range(len(peers)):
+        sq_copy(i).wait_recv()
+        sq = sq + sq_in[i]
+    scale = lax.rsqrt(sq[:, 0:1] / (HEADS * P_SIZE) + epsilon)
+    read_ref[...] = (gated * scale * gain_here).astype(BF16)[0:S]
+
+    for i in range(len(peers)):
+        sq_copy(i).wait_send()
+    for k in range(1, n):
+        log_copy(k).wait_send()
+        for g in range(steps):
+            state_copy(g, k).wait_send()
+
+    @pl.when(me < n - 1)
+    def _():
+        halo_copy().wait_send()
+
+    @pl.when(me == n - 1)
+    def _():
+        for k in range(1, n):
+            newest_copy(k).wait_send()
+
+
+def fused(*args):
+    x, wv, wk = args[0], args[2], args[4]
+    S, L, D = x.shape
+    n, m = lax.axis_size("sp"), lax.axis_size("tp")
+    F = wv.shape[1]
+    heads = F // P_SIZE
+    R = P_SIZE // n
+    G = next(g for g in (3, 2, 1) if S % g == 0)
+    steps = S // G
+    C, RH, SP = F + STATE, heads * R, 16
+    dims = (n, m, S, L, heads, R, G)
+    flat = list(args)
+    for i in (10, 11, 12):
+        flat[i] = args[i].reshape(1, HEADS)
+    hbm, vmem = pl.BlockSpec(memory_space=pl.ANY), pl.BlockSpec(memory_space=pltpu.VMEM)
+    specs = [hbm, vmem, hbm, hbm, hbm, hbm, hbm] + [vmem] * 7 + [hbm]
+    dma = pltpu.SemaphoreType.DMA
+    cache, read = pl.pallas_call(
+        lambda *refs: mixer_kernel(dims, *refs),
+        out_shape=(
+            jax.ShapeDtypeStruct((S, RH, STATE), BF16),
+            jax.ShapeDtypeStruct((S, RH), BF16),
+        ),
+        in_specs=specs,
+        out_specs=(vmem, vmem),
+        scratch_shapes=[
+            pltpu.VMEM((S, L, D), BF16),
+            pltpu.VMEM((S + 1, 16, D), BF16),
+            pltpu.VMEM((D, C + STATE), BF16),
+            pltpu.VMEM((D, STATE), BF16),
+            pltpu.VMEM((D, HEADS), BF16),
+            pltpu.VMEM((D, F), BF16),
+            pltpu.VMEM((S, L, HEADS), F32),
+            pltpu.VMEM((CONV, C + STATE), F32),
+            pltpu.VMEM((G, 8 + L, C), F32),
+            pltpu.VMEM((CONV - 1, SP, C), BF16),
+            pltpu.VMEM((CONV - 1, SP, C), BF16),
+            pltpu.VMEM((CONV - 1, SP, C), F32),
+            pltpu.VMEM((1, SP, C + STATE), F32),
+            pltpu.VMEM((SP, 128), F32),
+            pltpu.VMEM((n, SP, 128), F32),
+            pltpu.VMEM((n, S, RH, STATE), BF16),
+            pltpu.VMEM((n, S, RH, STATE), BF16),
+            pltpu.VMEM((SP, 128), F32),
+            pltpu.VMEM((n * m - 1, SP, 128), F32),
+            pltpu.VMEM((2 * HEADS, F), BF16),
+            dma((7,)),
+            dma((steps,)),
+            dma((2,)),
+            dma((n,)),
+            dma,
+            dma((steps, n)),
+            dma((steps, n)),
+            dma((n,)),
+            dma((n,)),
+            dma((n * m,)),
+            dma((n * m,)),
+        ],
+        compiler_params=pltpu.CompilerParams(
+            collective_id=0, has_side_effects=True, vmem_limit_bytes=56 * 1024 * 1024
+        ),
+    )(*flat)
+    return cache.reshape(S, heads, R, STATE), read.reshape(S, heads, R)
+
+
+def fits(n, m, shapes):
+    (S, L), F = shapes
+    heads, R = F // P_SIZE, P_SIZE // n
+    return (
+        n > 1
+        and F % 128 == 0
+        and R % 16 == 0
+        and (heads * R) % 128 == 0
+        and S <= 16
+        and L % 16 == 0
+        and L <= 128
+        and (HEADS // GROUPS) % heads == 0
+    )
+
+
+def part(*args):
+    shapes = (args[0].shape[:2], args[2].shape[1])
+    if fits(lax.axis_size("sp"), lax.axis_size("tp"), shapes):
+        return fused(*args)
+    return shards(*args)
+
+
 def solution(mesh):
     in_specs = (
         P("grp", "sp", None),
@@ -191,4 +622,4 @@
         P("grp", "sp", None),
     )
     out_specs = (P("grp", "tp", "sp", None), P("grp", "tp", "sp"))
-    return jax.shard_map(shards, mesh=mesh, in_specs=in_specs, out_specs=out_specs, check_vma=False)
+    return jax.shard_map(part, mesh=mesh, in_specs=in_specs, out_specs=out_specs, check_vma=False)

time: 184 us -> 64.5 us (0.35)
  blocking collectives: 68.4 us -> 0 us
  Pallas kernels: 0 us -> 56.4 us
  waiting for transfers between devices: 33.7 us -> 0 us
  other arithmetic: 24 us -> 0 us
  matrix products: 18.2 us -> 0 us
  between operations: 14.4 us -> 0.64 us
  local copies, waits for them, and re-layouts: 19.5 us -> 7.14 us
  starting transfers between devices: 5.01 us -> 0 us
    pallas_call x0 -> x1, Pallas kernels: none -> 56.4 us  [fused(): pl.pallas_call(lambda *refs: mixer_kernel(dims, *refs), out_shape=(jax.Sh...]
    psum x2 -> x0, blocking collectives: 54.8 us -> none  [the longest x1 32 us: shards(): squares = lax.psum(jnp.sum(gated * gated, axis=(1, 2)), ('sp', 'tp'))]
    reduce_scatter x1 -> x0, waiting for transfers between devices: 33.7 us -> none  [shards(): own_rows = lax.psum_scatter(scaled, 'sp', scatter_dimension=2, tiled=True)]
    dot_general x6 -> x0, matrix products: 18.2 us -> none  [the longest x1 8.94 us: shards(): jnp.dot(token_rows, weights_here, preferred_element_type=jnp.float32)]
    convert_element_type x8 -> x0, other arithmetic: 15.8 us -> none  [the longest x1 7.27 us: shards(): mixed = jax.nn.silu(total).astype(jnp.bfloat16)]
    all_gather x1 -> x0, blocking collectives: 13.6 us -> none  [prefix(): everything = lax.all_gather(shard, axis)]
    convert_element_type x2 -> x0, local copies, waits for them, and re-layouts: 9.9 us -> none  [the longest x1 5.6 us: shards(): head_input.astype(jnp.float32) * decay_weight[..., None]]
    ppermute x1 -> x0, starting transfers between devices: 4.97 us -> none  [shifted(): return lax.ppermute(block, axis, route)]
  transfers between devices with their start and end apart: 2 -> 0, of which waited for: 1 -> 0; matrix products, arithmetic and copies ran while one was open for 11% -> 0% of each run, Pallas kernels for 0% -> 0%
where the time goes in v1:
time: 64.5 us; the launch traced here: 64.2 us
  Pallas kernels  56.4 us (87%)
  local copies, waits for them, and re-layouts  7.14 us (11%)
    pallas_call x1, Pallas kernels, fused(): pl.pallas_call(lambda *refs: mixer_kernel(dims, *refs), out_shape=(jax.Sh...  56.4 us
    unnamed x3, local copies, waits for them, and re-layouts  5.76 us
    reshape x1, local copies, waits for them, and re-layouts, fused(): return (cache.reshape(S, heads, R, STATE), read.reshape(S, heads, R))  1.38 us

profile of v1, /device:TPU:0, one launch (start us, length us, event | category | flops | bytes accessed | tf_op | source)
XLA Modules:
  0.0 64.2 jit_solution(13352061243971895579)
XLA Ops:
  0.6 1.9 %copy.17.refs_6_ = bf16[2048,32]{1,0:T(8,128)(2,1)} copy(bf16[2048,32]{0,1:T(8,128)(2,1)} %param.21) | data formatting | bytes 262144 | tf_op args[6]
  2.5 2.1 %copy.18.refs_14_ = f32[12,128,32]{2,1,0:T(8,128)} copy(f32[12,128,32]{1,2,0:T(8,128)} %param.29) | data formatting | bytes 393216 | tf_op args[14]
  4.6 56.4 %shard_map.158 = (bf16[12,128,128]{2,1,0:T(8,128)(2,1)}, bf16[12,128]{1,0:T(8,128)(2,1)}) custom-call(bf16[12,128,2048]{2,1,0:T(8,128)(2,1)} %refs_0_.1, bf16[12,2048]{1,0:T(8,128)(2,1)} %refs_1_.1, bf16[2048,512]{1,0:T(8,128)(2,1)} %refs_2_.1, bf16[2048,512]{1,0:T(8,128)(2,1)} %refs_3_.1, bf16[2048,256]{1,0:T(8,128)(2,1)} %refs_4_.1, ...), custom_call_target="tpu_custom_call" | custom-call | tf_op jit(solution)/shard_map/pallas_call | solution.py:536
  61.1 1.4 %reshape.23 = bf16[12,8,16]{2,1,0:T(8,128)(2,1)} reshape(bf16[12,128]{1,0:T(8,128)(2,1)} %get-tuple-element.5) | data formatting | bytes 6144 | tf_op jit(solution)/shard_map/reshape | solution.py:581
  62.4 1.8 %copy.20 = bf16[12,8,16,128]{3,2,1,0:T(8,128)(2,1)} copy(bf16[12,8,16,128]{3,2,1,0:T(8,128)(2,1)} %bitcast.4) | data formatting | bytes 786432

commit v2 on v1

--- a/solution.py
+++ b/solution.py
@@ -295,7 +295,6 @@
     taps[:, C : C + STATE] = tq_ref[:, pl.ds(gcol, STATE)].astype(F32)
     edge[S] = jnp.zeros(edge.shape[1:], BF16)
     edge[S, 0:S, :] = next_ref[...]
-    logs_out[...] = jnp.zeros_like(logs_out)
     halo_out[...] = jnp.zeros_like(halo_out)
     newest_zero = jnp.zeros(newest.shape[1:], F32)
     head_of = ones_where((HEADS, F), lambda i, c: i == lead + lax.div(c, P_SIZE), BF16)
@@ -303,12 +302,19 @@
     expand[HEADS : 2 * HEADS, :] = head_of
     bias = bias_ref[...]
     speed = jnp.exp(speed_ref[...])
+    square = jnp.zeros((128, 128 - HEADS), F32)
+
+    def columns(row):
+        full = jnp.concatenate([jnp.broadcast_to(row, (128, HEADS)), square], axis=1)
+        return full.T[0:HEADS]
+
+    bias_t, speed_t = columns(bias), columns(speed)
 
     for c in first:
         c.wait()
     wall[:, C : C + STATE] = jnp.concatenate(
-        [ws[...], jnp.zeros((ws.shape[0], STATE - HEADS), BF16)], axis=1
-    )
+        [ws[...], jnp.zeros((STATE - HEADS, ws.shape[1]), BF16)], axis=0
+    ).T
     rows = edge[...].reshape((S + 1) * 16, edge.shape[2])
     eproj = jnp.dot(rows, wall[...], preferred_element_type=F32).astype(BF16).astype(F32)
     eq = jnp.dot(rows, wq[...], preferred_element_type=F32).astype(BF16).astype(F32)
@@ -357,8 +363,18 @@
             device_id_type=MESH,
         )
 
+    def log_copy(g, k):
+        return pltpu.make_async_remote_copy(
+            logs_out.at[pl.ds(g * G, G)],
+            logs.at[me, pl.ds(g * G, G)],
+            log_send.at[g, k],
+            log_recv.at[g, k],
+            device_id=at(k),
+            device_id_type=MESH,
+        )
+
     off_load.wait()
-    later_ones = ones_where((L, L), lambda t, u: u > t)
+    later_ones = ones_where((L, L), lambda u, t: u > t)
 
     def step(g, carry):
         load_x(g).wait()
@@ -383,15 +399,19 @@
             for j in range(CONV - 1):
                 r = 8 - (CONV - 1) + j
                 pad[q, r : r + 1, :] = halo[j, pl.ds(p, 1), :]
-            dt = softplus(raw[:, C : C + HEADS] + bias)
-            ld = off[p] - speed * dt
-            suffix = exact_dot(later_ones, ld)
-            logs_out[pl.ds(p, 1), 0:HEADS] = suffix[0:1] + ld[0:1]
+            dt = softplus(raw[:, C : C + STATE].T[0:HEADS] + bias_t)
+            ld = off[p] - speed_t * dt
+            suffix = exact_dot(ld, later_ones)
+            own = jnp.broadcast_to(suffix[:, 0:1] + ld[:, 0:1], (HEADS, 128))
+            logs_out[p] = jnp.concatenate([own] * (128 // HEADS), axis=0).T[0:8]
             w = dt * jnp.exp(suffix)
             hi = w.astype(BF16)
             lo = (w - hi.astype(F32)).astype(BF16)
-            wide = jnp.dot(
-                jnp.concatenate([hi, lo], axis=1), expand[...], preferred_element_type=F32
+            wide = lax.dot_general(
+                jnp.concatenate([hi, lo], axis=0),
+                expand[...],
+                (((0,), (0,)), ((), ())),
+                preferred_element_type=F32,
             )
 
             def mixed(c):
@@ -414,18 +434,13 @@
                         b = hh * P_SIZE + d * R
                         sendbuf[d, p, h * R : (h + 1) * R, :] = share[b : b + R]
         for k in range(1, n):
+            log_copy(g, k).start()
+        for k in range(1, n):
             state_copy(g, k).start()
         return carry
 
     lax.fori_loop(0, steps, step, 0)
 
-    def log_copy(k):
-        return pltpu.make_async_remote_copy(
-            logs_out, logs.at[me], log_send.at[k], log_recv.at[k], device_id=at(k), device_id_type=MESH
-        )
-
-    for k in range(1, n):
-        log_copy(k).start()
     logs[me] = logs_out[...]
     recv[me] = sendbuf[me]
 
@@ -457,23 +472,19 @@
     new_out = new_mixed[:, C : C + STATE]
     both = jnp.sum(new_in * new_out.astype(F32), axis=1, keepdims=True)
 
-    for k in range(1, n):
-        log_copy(k).wait_recv()
-    later = jnp.zeros(logs_out.shape, F32)
-    factors = [None] * n
-    for s in reversed(range(n)):
-        factors[s] = exact_dot(head_rows, jnp.exp(later)[:, 0:HEADS], ((1,), (1,)))
-        later = later + logs[s]
-
     where_row = lax.broadcasted_iota(jnp.int32, (SP, RH), 0)
     y = jnp.zeros((SP, RH), F32)
     for g in range(steps):
         for k in range(1, n):
+            log_copy(g, k).wait_recv()
             state_copy(g, k).wait_recv()
         for p in range(g * G, (g + 1) * G):
-            tot = factors[0][:, p : p + 1] * recv[0, p].astype(F32)
-            for s in range(1, n):
-                tot = tot + factors[s][:, p : p + 1] * recv[s, p].astype(F32)
+            later = jnp.zeros((1, HEADS), F32)
+            tot = jnp.zeros((RH, STATE), F32)
+            for s in reversed(range(n)):
+                factor = jnp.sum(head_rows * jnp.exp(later), axis=1, keepdims=True)
+                tot = tot + factor * recv[s, p].astype(F32)
+                later = later + logs[s, p, 0:1, 0:HEADS]
             kept = tot.astype(BF16)
             cache_ref[p] = kept
             part = lax.dot_general(
@@ -502,8 +513,8 @@
     for i in range(len(peers)):
         sq_copy(i).wait_send()
     for k in range(1, n):
-        log_copy(k).wait_send()
         for g in range(steps):
+            log_copy(g, k).wait_send()
             state_copy(g, k).wait_send()
 
     @pl.when(me < n - 1)
@@ -523,13 +534,15 @@
     F = wv.shape[1]
     heads = F // P_SIZE
     R = P_SIZE // n
-    G = next(g for g in (3, 2, 1) if S % g == 0)
+    G = next(g for g in (2, 3, 1) if S % g == 0)
     steps = S // G
     C, RH, SP = F + STATE, heads * R, 16
     dims = (n, m, S, L, heads, R, G)
     flat = list(args)
     for i in (10, 11, 12):
         flat[i] = args[i].reshape(1, HEADS)
+    flat[6] = args[6].T
+    flat[14] = jnp.swapaxes(args[14], 1, 2)
     hbm, vmem = pl.BlockSpec(memory_space=pl.ANY), pl.BlockSpec(memory_space=pltpu.VMEM)
     specs = [hbm, vmem, hbm, hbm, hbm, hbm, hbm] + [vmem] * 7 + [hbm]
     dma = pltpu.SemaphoreType.DMA
@@ -546,17 +559,17 @@
             pltpu.VMEM((S + 1, 16, D), BF16),
             pltpu.VMEM((D, C + STATE), BF16),
             pltpu.VMEM((D, STATE), BF16),
-            pltpu.VMEM((D, HEADS), BF16),
+            pltpu.VMEM((HEADS, D), BF16),
             pltpu.VMEM((D, F), BF16),
-            pltpu.VMEM((S, L, HEADS), F32),
+            pltpu.VMEM((S, HEADS, L), F32),
             pltpu.VMEM((CONV, C + STATE), F32),
             pltpu.VMEM((G, 8 + L, C), F32),
             pltpu.VMEM((CONV - 1, SP, C), BF16),
             pltpu.VMEM((CONV - 1, SP, C), BF16),
             pltpu.VMEM((CONV - 1, SP, C), F32),
             pltpu.VMEM((1, SP, C + STATE), F32),
-            pltpu.VMEM((SP, 128), F32),
-            pltpu.VMEM((n, SP, 128), F32),
+            pltpu.VMEM((S, 8, 128), F32),
+            pltpu.VMEM((n, S, 8, 128), F32),
             pltpu.VMEM((n, S, RH, STATE), BF16),
             pltpu.VMEM((n, S, RH, STATE), BF16),
             pltpu.VMEM((SP, 128), F32),
@@ -569,8 +582,8 @@
             dma,
             dma((steps, n)),
             dma((steps, n)),
-            dma((n,)),
-            dma((n,)),
+            dma((steps, n)),
+            dma((steps, n)),
             dma((n * m,)),
             dma((n * m,)),
         ],
@@ -591,7 +604,7 @@
         and (heads * R) % 128 == 0
         and S <= 16
         and L % 16 == 0
-        and L <= 128
+        and L == 128
         and (HEADS // GROUPS) % heads == 0
     )
 

time: 64.5 us -> 62.2 us (0.964)
  local copies, waits for them, and re-layouts: 7.14 us -> 3.14 us
  Pallas kernels: 56.4 us -> 58.1 us
    unnamed x3 -> x1, local copies, waits for them, and re-layouts: 5.76 us -> 1.77 us
    pallas_call x1, Pallas kernels: 56.4 us -> 58.1 us  [fused(): pl.pallas_call(lambda *refs: mixer_kernel(dims, *refs), out_shape=(jax.Sh...]
where the time goes in v2:
time: 62.2 us; the launch traced here: 61.9 us
  Pallas kernels  58.1 us (93%)
  local copies, waits for them, and re-layouts  3.14 us (5%)
  between operations  0.64 us (1%)
    pallas_call x1, Pallas kernels, fused(): pl.pallas_call(lambda *refs: mixer_kernel(dims, *refs), out_shape=(jax.Sh...  58.1 us
    unnamed x1, local copies, waits for them, and re-layouts  1.77 us
    reshape x1, local copies, waits for them, and re-layouts, fused(): return (cache.reshape(S, heads, R, STATE), read.reshape(S, heads, R))  1.37 us

profile of v2, /device:TPU:0, one launch (start us, length us, event | category | flops | bytes accessed | tf_op | source)
XLA Modules:
  0.0 61.9 jit_solution(5423331118877304753)
XLA Ops:
  0.6 58.1 %shard_map.158 = (bf16[12,128,128]{2,1,0:T(8,128)(2,1)}, bf16[12,128]{1,0:T(8,128)(2,1)}) custom-call(bf16[12,128,2048]{2,1,0:T(8,128)(2,1)} %refs_0_.1, bf16[12,2048]{1,0:T(8,128)(2,1)} %refs_1_.1, bf16[2048,512]{1,0:T(8,128)(2,1)} %refs_2_.1, bf16[2048,512]{1,0:T(8,128)(2,1)} %refs_3_.1, bf16[2048,256]{1,0:T(8,128)(2,1)} %refs_4_.1, ...), custom_call_target="tpu_custom_call" | custom-call | tf_op jit(solution)/shard_map/pallas_call | solution.py:549
  58.8 1.4 %reshape.23 = bf16[12,8,16]{2,1,0:T(8,128)(2,1)} reshape(bf16[12,128]{1,0:T(8,128)(2,1)} %get-tuple-element.5) | data formatting | bytes 6144 | tf_op jit(solution)/shard_map/reshape | solution.py:594
  60.2 1.8 %copy.18 = bf16[12,8,16,128]{3,2,1,0:T(8,128)(2,1)} copy(bf16[12,8,16,128]{3,2,1,0:T(8,128)(2,1)} %bitcast.6) | data formatting | bytes 786432
